TPU v7x, 512 devices: a whole 4x8x8 slice. The times are simulated.
512 devices in a mesh: sp: 32 (over z, x), tp: 16 (over y, core).
Axes of the slice: x: 4, y: 8, z: 8, core: 2. Of those that a mesh axis runs over, the one named last changes fastest.
Arguments:
- outer_gate: bfloat16 [8192, 2048], P('sp', 'tp'), may hold values from -6 to 6
- inner_gate: bfloat16 [8192, 2048], P('sp', 'tp'), may hold values from -6 to 6
- conv_input: bfloat16 [8192, 2048], P('sp', 'tp'), may hold values from -6 to 6
- conv_weight: bfloat16 [3, 2048], P(None, 'tp'), may hold values from -3.5 to 3.5
- doc_ids: int32 [8192], P('sp'), may hold values from 0 to 15, as said below
- output_weight: bfloat16 [2048, 4096], P(None, 'tp'), may hold values from -0.125 to 0.125
- residual: bfloat16 [8192, 4096], P('sp', 'tp'), as said below
- norm_gain: bfloat16 [4096], P('tp'), may hold values from 0.099609375 to 1.8984375
- expert_ids: int32 [8192, 2], P('sp'), may hold values from 0 to 31, all different within a row; in each aligned block of 256 rows (0 to 255, 256 to 511, ...) at most 32 rows name the same one
- group_weight: float32 [8192], P('sp'), may hold values from 0.25 to 1
- expert_weight: float32 [8192, 2], P('sp'), may hold values from 0.05 to 1
- gate_weight: bfloat16 [32, 4096, 2048], P('sp', None, 'tp'), may hold values from -0.09375 to 0.09375
- up_weight: bfloat16 [32, 4096, 2048], P('sp', None, 'tp'), may hold values from -0.09375 to 0.09375
- down_weight: bfloat16 [32, 2048, 4096], P('sp', None, 'tp'), may hold values from -0.125 to 0.125
Outputs:
- layer_out: bfloat16 [8192, 4096], P('sp', 'tp')
Inputs may be any that keep to these rules, and one draw needn't show every extreme that they name: `expert_ids`: within the 256 rows of one index of sp no expert is named more than 32 times, a bound that some block reaches; the two experts of a row differ. `doc_ids`: never falling along positions, rising by one at each document's start; every document has 256 to 768 positions, and one exactly 768. `residual`: Columns' scales are of order one to ten.
All inputs are finite; a program needn't handle non-finite values.
Results may differ from a plain program's by a relative error of at most 0.009.
Values may be sent and summed in bfloat16 or wider, within the bound.
A program may use at most 64 MiB of HBM per device.

v0:
```python
import jax
import jax.numpy as jnp
from jax import lax
from jax.sharding import PartitionSpec as P

EPS = 1e-06


def passed_along(value, axis, steps):
    count = lax.axis_size(axis)
    initial, last = (max(0, -steps), min(count, count - steps))
    return lax.ppermute(value, axis, [(source, source + steps) for source in range(initial, last)])


def from_everyone(x, axis):
    copies = jnp.broadcast_to(x, (lax.axis_size(axis), *x.shape))
    return lax.all_to_all(copies, axis, split_axis=0, concat_axis=0, tiled=True)


def joined_along(blocks, dim):
    dims = list(blocks.shape[1:])
    dims[dim] *= blocks.shape[0]
    return jnp.moveaxis(blocks, 0, dim).reshape(dims)


def collect(x, axis, dim):
    blocks = from_everyone(x, axis)
    return joined_along(blocks, dim)


def of_everyone(x, axis):
    everything = from_everyone(x, axis)
    return jnp.sum(everything, axis=0)


def per_device(
    outer_gate,
    inner_gate,
    conv_input,
    conv_weight,
    doc_ids,
    output_weight,
    residual,
    norm_gain,
    expert_ids,
    group_weight,
    expert_weight,
    gate_weight,
    up_weight,
    down_weight,
):
    row_count = conv_input.shape[0]
    products = inner_gate.astype(jnp.float32) * conv_input.astype(jnp.float32)
    own_docs = doc_ids.astype(jnp.float32)
    tail_rows, tail_docs = passed_along((products[-2:], own_docs[-2:]), "sp", 1)
    ext_products = jnp.concatenate([tail_rows, products], axis=0)
    ext_docs = jnp.concatenate([tail_docs, own_docs], axis=0)
    taps = conv_weight.astype(jnp.float32)
    conv = taps[2] * products
    for shift_by in (1, 2):
        first = 2 - shift_by
        same_doc = (ext_docs[first : first + row_count] == own_docs)[:, None]
        conv = conv + jnp.where(
            same_doc, taps[2 - shift_by] * ext_products[first : first + row_count], 0.0
        )
    branch = (outer_gate.astype(jnp.float32) * conv).astype(jnp.bfloat16)
    cols_local = output_weight.shape[1]
    branch_sum = jnp.dot(
        collect(branch, "tp", 1), output_weight, preferred_element_type=jnp.float32
    )
    resid = (residual.astype(jnp.float32) + branch_sum).astype(jnp.bfloat16)
    resid_wide = resid.astype(jnp.float32)
    total_sq = of_everyone(jnp.sum(resid_wide * resid_wide, axis=1), "tp")
    width = cols_local * lax.axis_size("tp")
    scale = lax.rsqrt(total_sq / width + EPS)[:, None]
    normed = (resid_wide * scale * norm_gain.astype(jnp.float32)).astype(jnp.bfloat16)
    experts = lax.axis_size("sp")
    capacity = 4 * row_count // experts
    flat_experts = expert_ids.reshape(-1)
    onehot = (flat_experts[:, None] == jnp.arange(experts, dtype=jnp.int32)[None, :]).astype(
        jnp.int32
    )
    slot_rank = jnp.sum((jnp.cumsum(onehot, axis=0) - onehot) * onehot, axis=1)
    slot_index = flat_experts * capacity + slot_rank
    token_of = jnp.arange(2 * row_count, dtype=jnp.int32) // 2
    token_table = jnp.full((experts * capacity,), row_count, jnp.int32).at[slot_index].set(token_of)
    gate_local = gate_weight[0]
    up_local = up_weight[0]
    arrived_rows = experts * capacity
    padded = jnp.concatenate([normed, jnp.zeros((1, cols_local), jnp.bfloat16)], axis=0)
    outgoing = padded[token_table].reshape(experts, capacity, cols_local)
    arrived = lax.all_to_all(outgoing, "sp", split_axis=0, concat_axis=0, tiled=True).reshape(
        arrived_rows, cols_local
    )
    piece = lax.all_gather(arrived, "tp", axis=1, tiled=True)
    gate_val = jnp.dot(piece, gate_local, preferred_element_type=jnp.float32)
    up_val = jnp.dot(piece, up_local, preferred_element_type=jnp.float32)
    hidden = (jax.nn.silu(gate_val) * up_val).astype(jnp.bfloat16)
    down_local = down_weight[0]
    expert_out = jnp.dot(
        lax.all_gather(hidden, "tp", axis=1, tiled=True),
        down_local,
        preferred_element_type=jnp.float32,
    ).astype(jnp.bfloat16)
    returned = lax.all_to_all(
        expert_out.reshape(experts, capacity, cols_local),
        "sp",
        split_axis=0,
        concat_axis=0,
        tiled=True,
    )
    picked = (
        returned.reshape(arrived_rows, cols_local)[slot_index]
        .reshape(row_count, 2, cols_local)
        .astype(jnp.float32)
    )
    mix_weight = (
        group_weight[:, None] * expert_weight / jnp.sum(expert_weight, axis=1, keepdims=True)
    )
    routed_sum = jnp.sum(picked * mix_weight[:, :, None], axis=1)
    return (resid_wide + routed_sum).astype(jnp.bfloat16)


def solution(mesh):
    return jax.shard_map(
        per_device,
        mesh=mesh,
        in_specs=(
            P("sp", "tp"),
            P("sp", "tp"),
            P("sp", "tp"),
            P(None, "tp"),
            P("sp"),
            P(None, "tp"),
            P("sp", "tp"),
            P("tp"),
            P("sp", None),
            P("sp"),
            P("sp", None),
            P("sp", None, "tp"),
            P("sp", None, "tp"),
            P("sp", None, "tp"),
        ),
        out_specs=P("sp", "tp"),
        check_vma=False,
    )
```

profile of v0, /device:TPU:8, one launch (start us, length us, event | category | flops | bytes accessed | tf_op | source)
XLA Modules:
  0.0 263.7 jit_solution(17630297964401948509)
XLA Ops:
  6.5 0.0 copy-start
  6.5 0.0 copy-start.4
  6.5 0.8 convert_element_type.60
  7.4 0.1 slice.34
  7.4 3.4 %collective-permute-start = (f32[2]{0:T(128)S(1)}, f32[2]{0:T(128)S(1)}, u32[]{:S(2)}, u32[]{:S(2)}) collective-permute-start(f32[2]{0:T(128)S(1)} %slice.34), channel_id=1, source_target_pairs={{0,16},{16,32},{32,48},{48,64},{64,80},{80,96},{96,112},{112,128},... | collective-permute-start | bytes 32 | tf_op jit(solution)/shard_map/ppermute | solution.py:12
  10.8 0.9 convert_multiply_fusion
  11.7 3.4 %collective-permute-start.1 = (f32[2,128]{1,0:T(2,128)S(1)}, f32[2,128]{1,0:T(2,128)S(1)}, u32[]{:S(2)}, u32[]{:S(2)}) collective-permute-start(f32[2,128]{1,0:T(2,128)S(1)} %slice.48), channel_id=1, source_target_pairs={{0,16},{16,32},{32,48},{48,64},{64,80},{80,96},{96,112},{112,128},... | collective-permute-start | bytes 3080 | tf_op jit(solution)/shard_map/ppermute | solution.py:12
  15.1 0.7 convert_element_type.57
  15.8 0.0 collective-permute-done
  15.8 0.1 pad_maximum_fusion.1
  15.9 0.8 slice_compare_fusion.1
  16.7 0.0 collective-permute-done.1
  16.7 1.0 fusion.13
  17.7 0.1 copy.28
  17.8 1.1 broadcast_in_dim.44
  18.9 7.6 %all-to-all-start = ((bf16[16,256,128]{1,2,0:T(8,128)(2,1)}), bf16[16,256,128]{1,2,0:T(8,128)(2,1)S(1)}, u32[]{:S(2)}, u32[]{:S(2)}) async-start(bf16[16,256,128]{1,2,0:T(8,128)(2,1)} %broadcast_in_dim.44), calls=%async_computation | async-start | bytes 2097152 | tf_op jit(solution)/shard_map/all_to_all | solution.py:17
  26.4 0.8 copy.31
  27.2 0.1 eq.37
  27.4 0.1 eq.33
  27.5 1.2 reduce-window.6
  28.7 0.2 slice_reduce_fusion
  29.0 0.7 broadcast_multiply_fusion
  29.7 0.1 copy.30
  29.8 0.1 mul.115
  30.0 0.1 fusion.18
  30.1 2.4 scatter_custom_fusion
  32.5 18.5 %all-to-all-done = bf16[16,256,128]{1,2,0:T(8,128)(2,1)S(1)} async-done(((bf16[16,256,128]{1,2,0:T(8,128)(2,1)}), bf16[16,256,128]{1,2,0:T(8,128)(2,1)S(1)}, u32[]{:S(2)}, u32[]{:S(2)}) %all-to-all-start) | async-done | bytes 1048608 | tf_op jit(solution)/shard_map/all_to_all | solution.py:17
  51.0 1.8 multiply_reduce_fusion.1
  52.8 0.6 broadcast_in_dim.45
  53.5 6.8 %all-to-all-start.1 = ((f32[16,1,256]{2,1,0:T(1,128)}), f32[16,1,256]{2,1,0:T(1,128)S(1)}, u32[]{:S(2)}, u32[]{:S(2)}) async-start(f32[16,1,256]{2,1,0:T(1,128)} %broadcast_in_dim.45), calls=%async_computation.1 | async-start | bytes 32768 | tf_op jit(solution)/shard_map/all_to_all | solution.py:17
  60.3 0.0 all-gather.3.cloned.1.call-start
  60.3 0.7 convert_element_type.64
  61.0 5.5 %all-to-all-done.1 = f32[16,1,256]{2,1,0:T(1,128)S(1)} async-done(((f32[16,1,256]{2,1,0:T(1,128)}), f32[16,1,256]{2,1,0:T(1,128)S(1)}, u32[]{:S(2)}, u32[]{:S(2)}) %all-to-all-start.1) | async-done | bytes 16416 | tf_op jit(solution)/shard_map/all_to_all | solution.py:17
  66.6 0.1 multiply_convert_fusion
  66.7 3.9 %gather_fusion = bf16[1024,256]{1,0:T(8,128)(2,1)S(1)} fusion(bf16[257,256]{1,0:T(8,128)(2,1)S(1)} %concatenate.11, s32[1024]{0:T(1024)S(1)} %fusion.20), kind=kCustom, calls=%fused_computation | custom fusion | bytes 1052672 | tf_op jit(solution)/shard_map/gather | solution.py:91
  70.7 32.5 %all_to_all.21 = bf16[32,32,256]{2,1,0:T(8,128)(2,1)} all-to-all(bf16[32,32,256]{2,1,0:T(8,128)(2,1)S(1)} %bitcast.51), channel_id=1, replica_groups=mesh['sp'=32,'tp'=16] {'sp'}, dimensions={0} | all-to-all | bytes 1048576 | tf_op jit(solution)/shard_map/all_to_all | solution.py:92
  103.2 0.0 all-gather.3.cloned.1.call-update
  103.2 0.0 all-gather.5.cloned.1.call-start
  103.2 58.8 %all-gather.3.cloned.1.call-done = bf16[1024,4096]{1,0:T(8,128)(2,1)} async-done(((bf16[1024,256]{1,0:T(8,128)(2,1)}), bf16[1024,4096]{1,0:T(8,128)(2,1)}) %all-gather.3.cloned.1.call-update) | async-done | bytes 8388624 | tf_op jit(solution)/shard_map/all_gather | solution.py:95
  162.0 0.0 copy-done.4
  162.0 0.0 copy-start.3
  162.0 0.0 copy-start.5
  162.0 5.9 %fusion.5 = f32[1024,128]{1,0:T(8,128)S(1)} fusion(bf16[1024,4096]{1,0:T(8,128)(2,1)} %all-gather.3.cloned.1.call-done, bf16[1,4096,128]{2,1,0:T(8,128)(2,1)S(1)} %copy-done.4), kind=kOutput, calls=%fused_computation.11 | convolution fusion | flops 1073741824 | bytes 9961472 | tf_op jit(solution)/shard_map/dot_general | solution.py:96
  167.9 0.0 copy-done.3
  167.9 0.1 copy-done.5
  168.0 0.0 copy-start.1
  168.0 0.0 copy-start.2
  168.0 3.0 %fusion = bf16[1024,128]{1,0:T(8,128)(2,1)} fusion(bf16[1024,4096]{1,0:T(8,128)(2,1)S(1)} %copy-done.3, bf16[1,4096,128]{2,1,0:T(8,128)(2,1)S(1)} %copy-done.5, f32[1024,128]{1,0:T(8,128)S(1)} %fusion.5), kind=kOutput, calls=%fused_computation.5 | convolution fusion | flops 1074528256 | bytes 10223616 | tf_op jit(solution)/shard_map/dot_general | solution.py:97
  171.0 0.0 all-gather.5.cloned.1.call-update
  171.0 49.6 %all-gather.5.cloned.1.call-done = bf16[1024,2048]{1,0:T(8,128)(2,1)} async-done(((bf16[1024,128]{1,0:T(8,128)(2,1)}), bf16[1024,2048]{1,0:T(8,128)(2,1)}) %all-gather.5.cloned.1.call-update) | async-done | bytes 4194320 | tf_op jit(solution)/shard_map/all_gather | solution.py:101
  220.6 0.0 copy-done
  220.6 4.2 %convolution_convert_fusion = bf16[1024,256]{1,0:T(8,128)(2,1)} fusion(bf16[1024,2048]{1,0:T(8,128)(2,1)} %all-gather.5.cloned.1.call-done, bf16[1,2048,256]{2,1,0:T(8,128)(2,1)S(1)} %copy-done), kind=kOutput, calls=%fused_computation.3 | convolution fusion | flops 1074003968 | bytes 5767168 | tf_op jit(solution)/shard_map/dot_general | solution.py:100
  224.9 10.2 %all-to-all-start.3 = ((bf16[32,32,256]{2,1,0:T(8,128)(2,1)}), bf16[32,32,256]{2,1,0:T(8,128)(2,1)S(1)}, u32[]{:S(2)}, u32[]{:S(2)}) async-start(bf16[32,32,256]{2,1,0:T(8,128)(2,1)} %bitcast.13), calls=%async_computation.3 | async-start | bytes 1048576 | tf_op jit(solution)/shard_map/all_to_all | solution.py:105
  235.0 0.0 copy-done.1
  235.1 0.0 copy-done.2
  235.1 0.1 copy.34
  235.3 18.0 %all-to-all-done.3 = bf16[32,32,256]{2,1,0:T(8,128)(2,1)S(1)} async-done(((bf16[32,32,256]{2,1,0:T(8,128)(2,1)}), bf16[32,32,256]{2,1,0:T(8,128)(2,1)S(1)}, u32[]{:S(2)}, u32[]{:S(2)}) %all-to-all-start.3) | async-done | bytes 524320 | tf_op jit(solution)/shard_map/all_to_all | solution.py:105
  253.3 1.9 gather_fusion.1
  255.2 0.3 reshape.85
  255.5 0.7 multiply_reduce_fusion
  256.2 0.7 add_convert_fusion
  (14 shorter events, 0.2 us)
Async XLA Ops:
  6.5 214.1 %copy-start = (bf16[1,2048,256]{2,1,0:T(8,128)(2,1)S(1)}, bf16[1,2048,256]{2,1,0:T(8,128)(2,1)}, u32[]{:S(2)}) copy-start(bf16[1,2048,256]{2,1,0:T(8,128)(2,1)} %param.27) | copy-start | bytes 3145732
  6.5 155.5 %copy-start.4 = (bf16[1,4096,128]{2,1,0:T(8,128)(2,1)S(1)}, bf16[1,4096,128]{2,1,0:T(8,128)(2,1)}, u32[]{:S(2)}) copy-start(bf16[1,4096,128]{2,1,0:T(8,128)(2,1)} %param.25) | copy-start | bytes 3145732
  7.4 8.4 %collective-permute-start = (f32[2]{0:T(128)S(1)}, f32[2]{0:T(128)S(1)}, u32[]{:S(2)}, u32[]{:S(2)}) collective-permute-start(f32[2]{0:T(128)S(1)} %slice.34), channel_id=1, source_target_pairs={{0,16},{16,32},{32,48},{48,64},{64,80},{80,96},{96,112},{112,128},... | collective-permute-start | bytes 32 | tf_op jit(solution)/shard_map/ppermute | solution.py:12
  11.7 4.9 %collective-permute-start.1 = (f32[2,128]{1,0:T(2,128)S(1)}, f32[2,128]{1,0:T(2,128)S(1)}, u32[]{:S(2)}, u32[]{:S(2)}) collective-permute-start(f32[2,128]{1,0:T(2,128)S(1)} %slice.48), channel_id=1, source_target_pairs={{0,16},{16,32},{32,48},{48,64},{64,80},{80,96},{96,112},{112,128},... | collective-permute-start | bytes 3080 | tf_op jit(solution)/shard_map/ppermute | solution.py:12
  18.9 32.2 %all-to-all-start = ((bf16[16,256,128]{1,2,0:T(8,128)(2,1)}), bf16[16,256,128]{1,2,0:T(8,128)(2,1)S(1)}, u32[]{:S(2)}, u32[]{:S(2)}) async-start(bf16[16,256,128]{1,2,0:T(8,128)(2,1)} %broadcast_in_dim.44), calls=%async_computation | async-start | bytes 2097152 | tf_op jit(solution)/shard_map/all_to_all | solution.py:17
  53.5 13.1 %all-to-all-start.1 = ((f32[16,1,256]{2,1,0:T(1,128)}), f32[16,1,256]{2,1,0:T(1,128)S(1)}, u32[]{:S(2)}, u32[]{:S(2)}) async-start(f32[16,1,256]{2,1,0:T(1,128)} %broadcast_in_dim.45), calls=%async_computation.1 | async-start | bytes 32768 | tf_op jit(solution)/shard_map/all_to_all | solution.py:17
  60.3 101.7 %all-gather.3.cloned.1.call-start = ((), (), s32[]{:S(2)}) async-start(), calls=%async_computation.4 | async-start | bytes 8912896 | tf_op jit(solution)/shard_map/all_gather | solution.py:95
  103.2 117.4 %all-gather.5.cloned.1.call-start = ((), (), s32[]{:S(2)}) async-start(), calls=%async_computation.5 | async-start | bytes 4456448 | tf_op jit(solution)/shard_map/all_gather | solution.py:101
  162.0 5.9 %copy-start.3 = (bf16[1024,4096]{1,0:T(8,128)(2,1)S(1)}, bf16[1024,4096]{1,0:T(8,128)(2,1)}, u32[]{:S(2)}) copy-start(bf16[1024,4096]{1,0:T(8,128)(2,1)} %all-gather.3.cloned.1.call-done) | copy-start | bytes 25165828
  162.0 6.0 %copy-start.5 = (bf16[1,4096,128]{2,1,0:T(8,128)(2,1)S(1)}, bf16[1,4096,128]{2,1,0:T(8,128)(2,1)}, u32[]{:S(2)}) copy-start(bf16[1,4096,128]{2,1,0:T(8,128)(2,1)} %param.26) | copy-start | bytes 3145732
  168.0 67.1 %copy-start.1 = (f32[256,2]{0,1:T(2,128)S(1)}, f32[256,2]{0,1:T(2,128)}, u32[]{:S(2)}) copy-start(f32[256,2]{0,1:T(2,128)} %param.24) | copy-start | bytes 6148
  168.0 67.1 %copy-start.2 = (f32[256]{0:T(256)S(1)}, f32[256]{0:T(256)}, u32[]{:S(2)}) copy-start(f32[256]{0:T(256)} %param.23) | copy-start | bytes 3076
  224.9 28.4 %all-to-all-start.3 = ((bf16[32,32,256]{2,1,0:T(8,128)(2,1)}), bf16[32,32,256]{2,1,0:T(8,128)(2,1)S(1)}, u32[]{:S(2)}, u32[]{:S(2)}) async-start(bf16[32,32,256]{2,1,0:T(8,128)(2,1)} %bitcast.13), calls=%async_computation.3 | async-start | bytes 1048576 | tf_op jit(solution)/shard_map/all_to_all | solution.py:105
Sparse Core Ops, SparseCore 0:
  103.3 58.6 all-gather.2
  171.2 49.4 all-gather.4
where the time goes:
time: 264 us
  waiting for transfers between devices  150 us (57%)
  blocking collectives  32.5 us (12%)
  starting transfers between devices  31.4 us (12%)
  matrix products  14.9 us (6%)
  between operations  13.6 us (5%)
  local copies, waits for them, and re-layouts  12.4 us (5%)
  other arithmetic  8.46 us (3%)
    all_gather x1, waiting for transfers between devices, per_device(): piece = lax.all_gather(arrived, 'tp', axis=1, tiled=True)  58.8 us
    all_gather x1, waiting for transfers between devices, per_device(): lax.all_gather(hidden, 'tp', axis=1, tiled=True)  49.6 us
    all_to_all x1, blocking collectives, per_device(): lax.all_to_all(outgoing, 'sp', split_axis=0, concat_axis=0, tiled=True)  32.5 us
    all_to_all x2, waiting for transfers between devices, from_everyone(): return lax.all_to_all(copies, axis, split_axis=0, concat_axis=0, tiled=True)  24 us
    all_to_all x1, waiting for transfers between devices, per_device(): lax.all_to_all(expert_out.reshape(experts, capacity, cols_local), 'sp', s...  18 us
    all_to_all x2, starting transfers between devices, from_everyone(): return lax.all_to_all(copies, axis, split_axis=0, concat_axis=0, tiled=True)  14.4 us
    all_to_all x1, starting transfers between devices, per_device(): lax.all_to_all(expert_out.reshape(experts, capacity, cols_local), 'sp', s...  10.2 us
    ppermute x2, starting transfers between devices, passed_along(): lax.ppermute(value, axis, [(source, source + steps) for source in range(i...  6.78 us
  transfers between devices with their start and end apart: 7, of which 5 were waited for; matrix products, arithmetic and copies ran while one was open for 4% of the time, Pallas kernels for 0%

commit v1 on v0

--- a/solution.py
+++ b/solution.py
@@ -4,6 +4,27 @@
 from jax.sharding import PartitionSpec as P
 
 EPS = 1e-06
+
+
+def collect_2(array, axis, dim):
+    size, index, rows = (lax.axis_size(axis), lax.axis_index(axis), array.shape[dim])
+    right = [(i, (i + 1) % size) for i in range(size)]
+    left = [(i, (i - 1) % size) for i in range(size)]
+    result = jnp.zeros((*array.shape[:dim], size * rows, *array.shape[dim + 1 :]), array.dtype)
+    result = lax.dynamic_update_slice_in_dim(result, array, index * rows, axis=dim)
+    from_left = from_right = array
+    middle = size // 2
+    for step in range(1, middle + 1):
+        from_left = lax.ppermute(from_left, axis, right)
+        result = lax.dynamic_update_slice_in_dim(
+            result, from_left, (index - step) % size * rows, axis=dim
+        )
+        if step < size - middle:
+            from_right = lax.ppermute(from_right, axis, left)
+            result = lax.dynamic_update_slice_in_dim(
+                result, from_right, (index + step) % size * rows, axis=dim
+            )
+    return result
 
 
 def passed_along(value, axis, steps):
@@ -92,7 +113,7 @@
     arrived = lax.all_to_all(outgoing, "sp", split_axis=0, concat_axis=0, tiled=True).reshape(
         arrived_rows, cols_local
     )
-    piece = lax.all_gather(arrived, "tp", axis=1, tiled=True)
+    piece = collect_2(arrived, "tp", 1)
     gate_val = jnp.dot(piece, gate_local, preferred_element_type=jnp.float32)
     up_val = jnp.dot(piece, up_local, preferred_element_type=jnp.float32)
     hidden = (jax.nn.silu(gate_val) * up_val).astype(jnp.bfloat16)

time: 264 us -> 275 us (1.042)
  starting transfers between devices: 31.4 us -> 45.4 us
  local copies, waits for them, and re-layouts: 12.4 us -> 17.5 us
  waiting for transfers between devices: 150 us -> 145 us
  matrix products: 14.9 us -> 11.4 us
    all_gather x1 -> x0, waiting for transfers between devices: 58.8 us -> none  [per_device(): piece = lax.all_gather(arrived, 'tp', axis=1, tiled=True)]
    ppermute x0 -> x15, waiting for transfers between devices: none -> 52.1 us  [the longest x8 49 us: collect_2(): from_left = lax.ppermute(from_left, axis, right)]
    ppermute x0 -> x15, starting transfers between devices: none -> 14.1 us  [the longest x7 14.1 us: collect_2(): from_right = lax.ppermute(from_right, axis, left)]
    dynamic_update_slice x0 -> x16, local copies, waits for them, and re-layouts: none -> 4.16 us  [the longest x8 2.6 us: collect_2(): lax.dynamic_update_slice_in_dim(result, from_left, (index - step) % size...]
    dot_general x1, matrix products: 5.86 us -> 2.34 us  [per_device(): gate_val = jnp.dot(piece, gate_local, preferred_element_type=jnp.float32)]
  transfers between devices with their start and end apart: 7 -> 21, of which waited for: 5 -> 16; matrix products, arithmetic and copies ran while one was open for 4% -> 5% of each run, Pallas kernels for 0% -> 0%
where the time goes in v1:
time: 275 us; the launch traced here: 274 us
  waiting for transfers between devices  145 us (53%)
  starting transfers between devices  45.4 us (17%)
  blocking collectives  32.4 us (12%)
  local copies, waits for them, and re-layouts  17.5 us (6%)
  between operations  13.9 us (5%)
  matrix products  11.4 us (4%)
  other arithmetic  8.4 us (3%)
    all_gather x1, waiting for transfers between devices, per_device(): lax.all_gather(hidden, 'tp', axis=1, tiled=True)  50.7 us
    ppermute x8, waiting for transfers between devices, collect_2(): from_left = lax.ppermute(from_left, axis, right)  49 us
    all_to_all x1, blocking collectives, per_device(): lax.all_to_all(outgoing, 'sp', split_axis=0, concat_axis=0, tiled=True)  32.4 us
    all_to_all x2, waiting for transfers between devices, from_everyone(): return lax.all_to_all(copies, axis, split_axis=0, concat_axis=0, tiled=True)  24 us
    all_to_all x1, waiting for transfers between devices, per_device(): lax.all_to_all(expert_out.reshape(experts, capacity, cols_local), 'sp', s...  18 us
    all_to_all x2, starting transfers between devices, from_everyone(): return lax.all_to_all(copies, axis, split_axis=0, concat_axis=0, tiled=True)  14.4 us
    ppermute x7, starting transfers between devices, collect_2(): from_right = lax.ppermute(from_right, axis, left)  14.1 us
    all_to_all x1, starting transfers between devices, per_device(): lax.all_to_all(expert_out.reshape(experts, capacity, cols_local), 'sp', s...  10.2 us
  transfers between devices with their start and end apart: 21, of which 16 were waited for; matrix products, arithmetic and copies ran while one was open for 5% of the time, Pallas kernels for 0%

profile of v1, /device:TPU:8, one launch (start us, length us, event | category | flops | bytes accessed | tf_op | source)
XLA Modules:
  0.0 273.8 jit_solution(10590167379694517775)
XLA Ops:
  6.5 0.8 convert_element_type.60
  7.4 3.4 %collective-permute-start = (f32[2]{0:T(128)S(1)}, f32[2]{0:T(128)S(1)}, u32[]{:S(2)}, u32[]{:S(2)}) collective-permute-start(f32[2]{0:T(128)S(1)} %slice.34), channel_id=1, source_target_pairs={{0,16},{16,32},{32,48},{48,64},{64,80},{80,96},{96,112},{112,128},... | collective-permute-start | bytes 32 | tf_op jit(solution)/shard_map/ppermute | solution.py:33
  10.8 0.9 convert_multiply_fusion
  11.7 3.4 %collective-permute-start.1 = (f32[2,128]{1,0:T(2,128)S(1)}, f32[2,128]{1,0:T(2,128)S(1)}, u32[]{:S(2)}, u32[]{:S(2)}) collective-permute-start(f32[2,128]{1,0:T(2,128)S(1)} %slice.48), channel_id=1, source_target_pairs={{0,16},{16,32},{32,48},{48,64},{64,80},{80,96},{96,112},{112,128},... | collective-permute-start | bytes 3080 | tf_op jit(solution)/shard_map/ppermute | solution.py:33
  15.1 0.7 convert_element_type.57
  15.8 0.1 pad_maximum_fusion.1
  15.9 0.8 slice_compare_fusion.1
  16.6 1.0 fusion.13
  17.6 0.1 copy.28
  17.7 1.1 broadcast_in_dim.47
  18.8 7.6 %all-to-all-start = ((bf16[16,256,128]{1,2,0:T(8,128)(2,1)}), bf16[16,256,128]{1,2,0:T(8,128)(2,1)S(1)}, u32[]{:S(2)}, u32[]{:S(2)}) async-start(bf16[16,256,128]{1,2,0:T(8,128)(2,1)} %broadcast_in_dim.47), calls=%async_computation | async-start | bytes 2097152 | tf_op jit(solution)/shard_map/all_to_all | solution.py:38
  26.4 0.8 copy.31
  27.2 0.1 eq.53
  27.3 0.1 eq.49
  27.5 1.2 reduce-window.6
  28.6 0.2 slice_reduce_fusion
  28.9 0.7 broadcast_multiply_fusion
  29.6 0.1 copy.30
  29.7 0.1 mul.163
  29.9 0.1 fusion.18
  30.0 2.4 scatter_custom_fusion
  32.5 18.5 %all-to-all-done = bf16[16,256,128]{1,2,0:T(8,128)(2,1)S(1)} async-done(((bf16[16,256,128]{1,2,0:T(8,128)(2,1)}), bf16[16,256,128]{1,2,0:T(8,128)(2,1)S(1)}, u32[]{:S(2)}, u32[]{:S(2)}) %all-to-all-start) | async-done | bytes 1048608 | tf_op jit(solution)/shard_map/all_to_all | solution.py:38
  51.0 1.8 multiply_reduce_fusion.1
  52.8 0.6 broadcast_in_dim.49
  53.4 6.8 %all-to-all-start.1 = ((f32[16,1,256]{2,1,0:T(1,128)}), f32[16,1,256]{2,1,0:T(1,128)S(1)}, u32[]{:S(2)}, u32[]{:S(2)}) async-start(f32[16,1,256]{2,1,0:T(1,128)} %broadcast_in_dim.49), calls=%async_computation.1 | async-start | bytes 32768 | tf_op jit(solution)/shard_map/all_to_all | solution.py:38
  60.3 0.7 convert_element_type.64
  60.9 5.5 %all-to-all-done.1 = f32[16,1,256]{2,1,0:T(1,128)S(1)} async-done(((f32[16,1,256]{2,1,0:T(1,128)}), f32[16,1,256]{2,1,0:T(1,128)S(1)}, u32[]{:S(2)}, u32[]{:S(2)}) %all-to-all-start.1) | async-done | bytes 16416 | tf_op jit(solution)/shard_map/all_to_all | solution.py:38
  66.5 0.1 multiply_convert_fusion.1
  66.6 3.9 %gather_fusion = bf16[1024,256]{1,0:T(8,128)(2,1)S(1)} fusion(bf16[257,256]{1,0:T(8,128)(2,1)S(1)} %concatenate.11, s32[1024]{0:T(1024)S(1)} %fusion.20), kind=kCustom, calls=%fused_computation | custom fusion | bytes 1052672 | tf_op jit(solution)/shard_map/gather | solution.py:112
  70.6 32.4 %all_to_all.21 = bf16[32,32,256]{2,1,0:T(8,128)(2,1)S(1)} all-to-all(bf16[32,32,256]{2,1,0:T(8,128)(2,1)S(1)} %bitcast.55), channel_id=1, replica_groups=mesh['sp'=32,'tp'=16] {'sp'}, dimensions={0} | all-to-all | bytes 1048576 | tf_op jit(solution)/shard_map/all_to_all | solution.py:113
  103.0 1.7 collective-permute-start.3
  104.7 6.9 %collective-permute-done.2 = bf16[1024,256]{1,0:T(8,128)(2,1)S(1)} collective-permute-done((bf16[1024,256]{1,0:T(8,128)(2,1)S(1)}, bf16[1024,256]{1,0:T(8,128)(2,1)S(1)}, u32[]{:S(2)}, u32[]{:S(2)}) %collective-permute-start.2) | collective-permute-done | bytes 524320 | tf_op jit(solution)/shard_map/ppermute | solution.py:18
  111.6 2.0 collective-permute-start.5
  113.6 6.6 %collective-permute-done.4 = bf16[1024,256]{1,0:T(8,128)(2,1)S(1)} collective-permute-done((bf16[1024,256]{1,0:T(8,128)(2,1)S(1)}, bf16[1024,256]{1,0:T(8,128)(2,1)S(1)}, u32[]{:S(2)}, u32[]{:S(2)}) %collective-permute-start.4) | collective-permute-done | bytes 524320 | tf_op jit(solution)/shard_map/ppermute | solution.py:18
  120.2 0.1 collective-permute-done.5
  120.3 2.2 collective-permute-start.7
  122.5 6.3 %collective-permute-done.6 = bf16[1024,256]{1,0:T(8,128)(2,1)S(1)} collective-permute-done((bf16[1024,256]{1,0:T(8,128)(2,1)S(1)}, bf16[1024,256]{1,0:T(8,128)(2,1)S(1)}, u32[]{:S(2)}, u32[]{:S(2)}) %collective-permute-start.6) | collective-permute-done | bytes 524320 | tf_op jit(solution)/shard_map/ppermute | solution.py:18
  128.8 0.4 collective-permute-done.7
  129.2 2.2 collective-permute-start.9
  131.4 6.1 %collective-permute-done.8 = bf16[1024,256]{1,0:T(8,128)(2,1)} collective-permute-done((bf16[1024,256]{1,0:T(8,128)(2,1)S(1)}, bf16[1024,256]{1,0:T(8,128)(2,1)}, u32[]{:S(2)}, u32[]{:S(2)}) %collective-permute-start.8) | collective-permute-done | bytes 524320 | tf_op jit(solution)/shard_map/ppermute | solution.py:18
  137.5 0.6 collective-permute-done.9
  138.1 2.3 collective-permute-start.11
  140.5 6.0 %collective-permute-done.10 = bf16[1024,256]{1,0:T(8,128)(2,1)} collective-permute-done((bf16[1024,256]{1,0:T(8,128)(2,1)}, bf16[1024,256]{1,0:T(8,128)(2,1)}, u32[]{:S(2)}, u32[]{:S(2)}) %collective-permute-start.10) | collective-permute-done | bytes 524320 | tf_op jit(solution)/shard_map/ppermute | solution.py:18
  146.4 1.0 broadcast_in_dim.48
  147.8 1.8 collective-permute-start.13
  149.7 5.5 %collective-permute-done.12 = bf16[1024,256]{1,0:T(8,128)(2,1)S(1)} collective-permute-done((bf16[1024,256]{1,0:T(8,128)(2,1)}, bf16[1024,256]{1,0:T(8,128)(2,1)S(1)}, u32[]{:S(2)}, u32[]{:S(2)}) %collective-permute-start.12) | collective-permute-done | bytes 524320 | tf_op jit(solution)/shard_map/ppermute | solution.py:18
  155.4 1.1 constant_dynamic-update-slice_fusion.8
  156.5 1.1 constant_dynamic-update-slice_fusion.7
  157.7 1.8 collective-permute-start.15
  159.4 1.1 constant_dynamic-update-slice_fusion.6
  160.5 3.4 %collective-permute-done.14 = bf16[1024,256]{1,0:T(8,128)(2,1)S(1)} collective-permute-done((bf16[1024,256]{1,0:T(8,128)(2,1)S(1)}, bf16[1024,256]{1,0:T(8,128)(2,1)S(1)}, u32[]{:S(2)}, u32[]{:S(2)}) %collective-permute-start.14) | collective-permute-done | bytes 524320 | tf_op jit(solution)/shard_map/ppermute | solution.py:18
  164.2 1.9 collective-permute-done.15
  166.2 8.3 %collective-permute-done.16 = bf16[1024,256]{1,0:T(8,128)(2,1)S(1)} collective-permute-done((bf16[1024,256]{1,0:T(8,128)(2,1)S(1)}, bf16[1024,256]{1,0:T(8,128)(2,1)S(1)}, u32[]{:S(2)}, u32[]{:S(2)}) %collective-permute-start.16) | collective-permute-done | bytes 524320 | tf_op jit(solution)/shard_map/ppermute | solution.py:18
  174.6 2.3 fusion.5
  177.0 3.0 %multiply_convert_fusion = bf16[1024,128]{1,0:T(8,128)(2,1)} fusion(f32[1024,128]{1,0:T(8,128)S(1)} %fusion.5, bf16[1024,4096]{1,0:T(8,128)(2,1)S(1)} %constant_dynamic-update-slice_fusion, bf16[1,4096,128]{2,1,0:T(8,128)(2,1)S(1)} %copy-done.12), kind=kOutput, calls=%fused_computation.13 | convolution fusion | flops 1074528256 | bytes 10223616 | tf_op jit(solution)/shard_map/dot_general | solution.py:118
  180.0 50.7 %all-gather.2.cloned.1.call-done = bf16[1024,2048]{1,0:T(8,128)(2,1)} async-done(((bf16[1024,128]{1,0:T(8,128)(2,1)}), bf16[1024,2048]{1,0:T(8,128)(2,1)}) %all-gather.2.cloned.1.call-update) | async-done | bytes 4194320 | tf_op jit(solution)/shard_map/all_gather | solution.py:122
  230.7 4.2 %convolution_convert_fusion = bf16[1024,256]{1,0:T(8,128)(2,1)} fusion(bf16[1024,2048]{1,0:T(8,128)(2,1)} %all-gather.2.cloned.1.call-done, bf16[1,2048,256]{2,1,0:T(8,128)(2,1)S(1)} %copy-done), kind=kOutput, calls=%fused_computation.3 | convolution fusion | flops 1074003968 | bytes 5767168 | tf_op jit(solution)/shard_map/dot_general | solution.py:121
  235.0 10.2 %all-to-all-start.3 = ((bf16[32,32,256]{2,1,0:T(8,128)(2,1)}), bf16[32,32,256]{2,1,0:T(8,128)(2,1)S(1)}, u32[]{:S(2)}, u32[]{:S(2)}) async-start(bf16[32,32,256]{2,1,0:T(8,128)(2,1)} %bitcast.13), calls=%async_computation.3 | async-start | bytes 1048576 | tf_op jit(solution)/shard_map/all_to_all | solution.py:126
  245.2 0.1 copy.34
  245.4 18.0 %all-to-all-done.3 = bf16[32,32,256]{2,1,0:T(8,128)(2,1)S(1)} async-done(((bf16[32,32,256]{2,1,0:T(8,128)(2,1)}), bf16[32,32,256]{2,1,0:T(8,128)(2,1)S(1)}, u32[]{:S(2)}, u32[]{:S(2)}) %all-to-all-start.3) | async-done | bytes 524320 | tf_op jit(solution)/shard_map/all_to_all | solution.py:126
  263.4 1.9 gather_fusion.1
  265.3 0.3 reshape.85
  265.6 0.7 multiply_reduce_fusion
  266.3 0.7 add_convert_fusion
  (69 shorter events, 1.2 us)
Async XLA Ops:
  6.5 224.2 %copy-start = (bf16[1,2048,256]{2,1,0:T(8,128)(2,1)S(1)}, bf16[1,2048,256]{2,1,0:T(8,128)(2,1)}, u32[]{:S(2)}) copy-start(bf16[1,2048,256]{2,1,0:T(8,128)(2,1)} %param.27) | copy-start | bytes 3145732
  7.4 8.4 %collective-permute-start = (f32[2]{0:T(128)S(1)}, f32[2]{0:T(128)S(1)}, u32[]{:S(2)}, u32[]{:S(2)}) collective-permute-start(f32[2]{0:T(128)S(1)} %slice.34), channel_id=1, source_target_pairs={{0,16},{16,32},{32,48},{48,64},{64,80},{80,96},{96,112},{112,128},... | collective-permute-start | bytes 32 | tf_op jit(solution)/shard_map/ppermute | solution.py:33
  11.7 4.9 %collective-permute-start.1 = (f32[2,128]{1,0:T(2,128)S(1)}, f32[2,128]{1,0:T(2,128)S(1)}, u32[]{:S(2)}, u32[]{:S(2)}) collective-permute-start(f32[2,128]{1,0:T(2,128)S(1)} %slice.48), channel_id=1, source_target_pairs={{0,16},{16,32},{32,48},{48,64},{64,80},{80,96},{96,112},{112,128},... | collective-permute-start | bytes 3080 | tf_op jit(solution)/shard_map/ppermute | solution.py:33
  18.8 32.2 %all-to-all-start = ((bf16[16,256,128]{1,2,0:T(8,128)(2,1)}), bf16[16,256,128]{1,2,0:T(8,128)(2,1)S(1)}, u32[]{:S(2)}, u32[]{:S(2)}) async-start(bf16[16,256,128]{1,2,0:T(8,128)(2,1)} %broadcast_in_dim.47), calls=%async_computation | async-start | bytes 2097152 | tf_op jit(solution)/shard_map/all_to_all | solution.py:38
  53.4 13.1 %all-to-all-start.1 = ((f32[16,1,256]{2,1,0:T(1,128)}), f32[16,1,256]{2,1,0:T(1,128)S(1)}, u32[]{:S(2)}, u32[]{:S(2)}) async-start(f32[16,1,256]{2,1,0:T(1,128)} %broadcast_in_dim.49), calls=%async_computation.1 | async-start | bytes 32768 | tf_op jit(solution)/shard_map/all_to_all | solution.py:38
  60.2 170.5 %all-gather.2.cloned.1.call-start = ((), (), s32[]{:S(2)}) async-start(), calls=%async_computation.4 | async-start | bytes 4456448 | tf_op jit(solution)/shard_map/all_gather | solution.py:122
  103.0 8.6 %collective-permute-start.2 = (bf16[1024,256]{1,0:T(8,128)(2,1)S(1)}, bf16[1024,256]{1,0:T(8,128)(2,1)S(1)}, u32[]{:S(2)}, u32[]{:S(2)}) collective-permute-start(bf16[1024,256]{1,0:T(8,128)(2,1)S(1)} %bitcast.52), channel_id=1, source_target_pairs={{0,1},{1,2},{2,3},{3,4},{4,5},{5,6},{6,7},{7,8},{8,9},{9,10},{10,1... | collective-permute-start | bytes 1572872 | tf_op jit(solution)/shard_map/ppermute | solution.py:18
  103.0 8.6 %collective-permute-start.3 = (bf16[1024,256]{1,0:T(8,128)(2,1)S(1)}, bf16[1024,256]{1,0:T(8,128)(2,1)S(1)}, u32[]{:S(2)}, u32[]{:S(2)}) collective-permute-start(bf16[1024,256]{1,0:T(8,128)(2,1)S(1)} %bitcast.53), channel_id=1, source_target_pairs={{0,15},{1,0},{2,1},{3,2},{4,3},{5,4},{6,5},{7,6},{8,7},{9,8},{10,9... | collective-permute-start | bytes 1572872 | tf_op jit(solution)/shard_map/ppermute | solution.py:23
  111.6 2.0 copy-start.3
  111.6 8.6 %collective-permute-start.4 = (bf16[1024,256]{1,0:T(8,128)(2,1)S(1)}, bf16[1024,256]{1,0:T(8,128)(2,1)S(1)}, u32[]{:S(2)}, u32[]{:S(2)}) collective-permute-start(bf16[1024,256]{1,0:T(8,128)(2,1)S(1)} %collective-permute-done.2), channel_id=1, source_target_pairs={{0,1},{1,2},{2,3},{3,4},{4,5},{5,6},{6,7},{7,8},{8,9},{9,10},{10,1... | collective-permute-start | bytes 1572872 | tf_op jit(solution)/shard_map/ppermute | solution.py:18
  111.6 26.5 %copy-start.5 = (bf16[1024,256]{1,0:T(8,128)(2,1)}, bf16[1024,256]{1,0:T(8,128)(2,1)S(1)}, u32[]{:S(2)}) copy-start(bf16[1024,256]{1,0:T(8,128)(2,1)S(1)} %collective-permute-done.3) | copy-start | bytes 1572868
  111.6 8.7 %collective-permute-start.5 = (bf16[1024,256]{1,0:T(8,128)(2,1)S(1)}, bf16[1024,256]{1,0:T(8,128)(2,1)S(1)}, u32[]{:S(2)}, u32[]{:S(2)}) collective-permute-start(bf16[1024,256]{1,0:T(8,128)(2,1)S(1)} %collective-permute-done.3), channel_id=1, source_target_pairs={{0,15},{1,0},{2,1},{3,2},{4,3},{5,4},{6,5},{7,6},{8,7},{9,8},{10,9... | collective-permute-start | bytes 1572872 | tf_op jit(solution)/shard_map/ppermute | solution.py:23
  120.2 20.3 %copy-start.7 = (bf16[1024,256]{1,0:T(8,128)(2,1)}, bf16[1024,256]{1,0:T(8,128)(2,1)S(1)}, u32[]{:S(2)}) copy-start(bf16[1024,256]{1,0:T(8,128)(2,1)S(1)} %collective-permute-done.4) | copy-start | bytes 1572868
  120.2 8.6 %collective-permute-start.6 = (bf16[1024,256]{1,0:T(8,128)(2,1)S(1)}, bf16[1024,256]{1,0:T(8,128)(2,1)S(1)}, u32[]{:S(2)}, u32[]{:S(2)}) collective-permute-start(bf16[1024,256]{1,0:T(8,128)(2,1)S(1)} %collective-permute-done.4), channel_id=1, source_target_pairs={{0,1},{1,2},{2,3},{3,4},{4,5},{5,6},{6,7},{7,8},{8,9},{9,10},{10,1... | collective-permute-start | bytes 1572872 | tf_op jit(solution)/shard_map/ppermute | solution.py:18
  120.3 17.2 %copy-start.1 = (bf16[1024,256]{1,0:T(8,128)(2,1)}, bf16[1024,256]{1,0:T(8,128)(2,1)S(1)}, u32[]{:S(2)}) copy-start(bf16[1024,256]{1,0:T(8,128)(2,1)S(1)} %collective-permute-done.5) | copy-start | bytes 1572868
  120.3 8.9 %collective-permute-start.7 = (bf16[1024,256]{1,0:T(8,128)(2,1)S(1)}, bf16[1024,256]{1,0:T(8,128)(2,1)S(1)}, u32[]{:S(2)}, u32[]{:S(2)}) collective-permute-start(bf16[1024,256]{1,0:T(8,128)(2,1)S(1)} %collective-permute-done.5), channel_id=1, source_target_pairs={{0,15},{1,0},{2,1},{3,2},{4,3},{5,4},{6,5},{7,6},{8,7},{9,8},{10,9... | collective-permute-start | bytes 1572872 | tf_op jit(solution)/shard_map/ppermute | solution.py:23
  128.8 8.7 %collective-permute-start.8 = (bf16[1024,256]{1,0:T(8,128)(2,1)S(1)}, bf16[1024,256]{1,0:T(8,128)(2,1)}, u32[]{:S(2)}, u32[]{:S(2)}) collective-permute-start(bf16[1024,256]{1,0:T(8,128)(2,1)S(1)} %collective-permute-done.6), channel_id=1, source_target_pairs={{0,1},{1,2},{2,3},{3,4},{4,5},{5,6},{6,7},{7,8},{8,9},{9,10},{10,1... | collective-permute-start | bytes 1572872 | tf_op jit(solution)/shard_map/ppermute | solution.py:18
  129.2 8.9 %collective-permute-start.9 = (bf16[1024,256]{1,0:T(8,128)(2,1)S(1)}, bf16[1024,256]{1,0:T(8,128)(2,1)}, u32[]{:S(2)}, u32[]{:S(2)}) collective-permute-start(bf16[1024,256]{1,0:T(8,128)(2,1)S(1)} %collective-permute-done.7), channel_id=1, source_target_pairs={{0,15},{1,0},{2,1},{3,2},{4,3},{5,4},{6,5},{7,6},{8,7},{9,8},{10,9... | collective-permute-start | bytes 1572872 | tf_op jit(solution)/shard_map/ppermute | solution.py:23
  137.5 8.9 %collective-permute-start.10 = (bf16[1024,256]{1,0:T(8,128)(2,1)}, bf16[1024,256]{1,0:T(8,128)(2,1)}, u32[]{:S(2)}, u32[]{:S(2)}) collective-permute-start(bf16[1024,256]{1,0:T(8,128)(2,1)} %collective-permute-done.8), channel_id=1, source_target_pairs={{0,1},{1,2},{2,3},{3,4},{4,5},{5,6},{6,7},{7,8},{8,9},{9,10},{10,1... | collective-permute-start | bytes 1572872 | tf_op jit(solution)/shard_map/ppermute | solution.py:18
  138.1 9.7 %collective-permute-start.11 = (bf16[1024,256]{1,0:T(8,128)(2,1)}, bf16[1024,256]{1,0:T(8,128)(2,1)S(1)}, u32[]{:S(2)}, u32[]{:S(2)}) collective-permute-start(bf16[1024,256]{1,0:T(8,128)(2,1)} %collective-permute-done.9), channel_id=1, source_target_pairs={{0,15},{1,0},{2,1},{3,2},{4,3},{5,4},{6,5},{7,6},{8,7},{9,8},{10,9... | collective-permute-start | bytes 1572872 | tf_op jit(solution)/shard_map/ppermute | solution.py:23
  140.5 7.1 %copy-start.4 = (bf16[1024,256]{1,0:T(8,128)(2,1)S(1)}, bf16[1024,256]{1,0:T(8,128)(2,1)}, u32[]{:S(2)}) copy-start(bf16[1024,256]{1,0:T(8,128)(2,1)} %copy-done.3) | copy-start | bytes 1572868
  140.5 7.2 %copy-start.6 = (bf16[1024,256]{1,0:T(8,128)(2,1)S(1)}, bf16[1024,256]{1,0:T(8,128)(2,1)}, u32[]{:S(2)}) copy-start(bf16[1024,256]{1,0:T(8,128)(2,1)} %copy-done.5) | copy-start | bytes 1572868
  140.5 7.3 %copy-start.8 = (bf16[1024,256]{1,0:T(8,128)(2,1)S(1)}, bf16[1024,256]{1,0:T(8,128)(2,1)}, u32[]{:S(2)}) copy-start(bf16[1024,256]{1,0:T(8,128)(2,1)} %copy-done.7) | copy-start | bytes 1572868
  140.5 9.2 %copy-start.2 = (bf16[1024,256]{1,0:T(8,128)(2,1)S(1)}, bf16[1024,256]{1,0:T(8,128)(2,1)}, u32[]{:S(2)}) copy-start(bf16[1024,256]{1,0:T(8,128)(2,1)} %copy-done.1) | copy-start | bytes 1572868
  146.4 8.8 %collective-permute-start.12 = (bf16[1024,256]{1,0:T(8,128)(2,1)}, bf16[1024,256]{1,0:T(8,128)(2,1)S(1)}, u32[]{:S(2)}, u32[]{:S(2)}) collective-permute-start(bf16[1024,256]{1,0:T(8,128)(2,1)} %collective-permute-done.10), channel_id=1, source_target_pairs={{0,1},{1,2},{2,3},{3,4},{4,5},{5,6},{6,7},{7,8},{8,9},{9,10},{10,1... | collective-permute-start | bytes 1572872 | tf_op jit(solution)/shard_map/ppermute | solution.py:18
  147.5 27.1 %copy-start.11 = (bf16[1,4096,128]{2,1,0:T(8,128)(2,1)S(1)}, bf16[1,4096,128]{2,1,0:T(8,128)(2,1)}, u32[]{:S(2)}) copy-start(bf16[1,4096,128]{2,1,0:T(8,128)(2,1)} %param.25) | copy-start | bytes 3145732
  147.8 9.8 %collective-permute-start.13 = (bf16[1024,256]{1,0:T(8,128)(2,1)S(1)}, bf16[1024,256]{1,0:T(8,128)(2,1)S(1)}, u32[]{:S(2)}, u32[]{:S(2)}) collective-permute-start(bf16[1024,256]{1,0:T(8,128)(2,1)S(1)} %collective-permute-done.11), channel_id=1, source_target_pairs={{0,15},{1,0},{2,1},{3,2},{4,3},{5,4},{6,5},{7,6},{8,7},{9,8},{10,9... | collective-permute-start | bytes 1572872 | tf_op jit(solution)/shard_map/ppermute | solution.py:23
  155.3 8.6 %collective-permute-start.14 = (bf16[1024,256]{1,0:T(8,128)(2,1)S(1)}, bf16[1024,256]{1,0:T(8,128)(2,1)S(1)}, u32[]{:S(2)}, u32[]{:S(2)}) collective-permute-start(bf16[1024,256]{1,0:T(8,128)(2,1)S(1)} %collective-permute-done.12), channel_id=1, source_target_pairs={{0,1},{1,2},{2,3},{3,4},{4,5},{5,6},{6,7},{7,8},{8,9},{9,10},{10,1... | collective-permute-start | bytes 1572872 | tf_op jit(solution)/shard_map/ppermute | solution.py:18
  157.7 8.5 %collective-permute-start.15 = (bf16[1024,256]{1,0:T(8,128)(2,1)S(1)}, bf16[1024,256]{1,0:T(8,128)(2,1)S(1)}, u32[]{:S(2)}, u32[]{:S(2)}) collective-permute-start(bf16[1024,256]{1,0:T(8,128)(2,1)S(1)} %collective-permute-done.13), channel_id=1, source_target_pairs={{0,15},{1,0},{2,1},{3,2},{4,3},{5,4},{6,5},{7,6},{8,7},{9,8},{10,9... | collective-permute-start | bytes 1572872 | tf_op jit(solution)/shard_map/ppermute | solution.py:23
  163.9 10.6 %collective-permute-start.16 = (bf16[1024,256]{1,0:T(8,128)(2,1)S(1)}, bf16[1024,256]{1,0:T(8,128)(2,1)S(1)}, u32[]{:S(2)}, u32[]{:S(2)}) collective-permute-start(bf16[1024,256]{1,0:T(8,128)(2,1)S(1)} %collective-permute-done.14), channel_id=1, source_target_pairs={{0,1},{1,2},{2,3},{3,4},{4,5},{5,6},{6,7},{7,8},{8,9},{9,10},{10,1... | collective-permute-start | bytes 1572872 | tf_op jit(solution)/shard_map/ppermute | solution.py:18
  163.9 13.0 %copy-start.12 = (bf16[1,4096,128]{2,1,0:T(8,128)(2,1)S(1)}, bf16[1,4096,128]{2,1,0:T(8,128)(2,1)}, u32[]{:S(2)}) copy-start(bf16[1,4096,128]{2,1,0:T(8,128)(2,1)} %param.26) | copy-start | bytes 3145732
  177.0 68.2 %copy-start.9 = (f32[256,2]{0,1:T(2,128)S(1)}, f32[256,2]{0,1:T(2,128)}, u32[]{:S(2)}) copy-start(f32[256,2]{0,1:T(2,128)} %param.24) | copy-start | bytes 6148
  177.0 68.2 %copy-start.10 = (f32[256]{0:T(256)S(1)}, f32[256]{0:T(256)}, u32[]{:S(2)}) copy-start(f32[256]{0:T(256)} %param.23) | copy-start | bytes 3076
  235.0 28.4 %all-to-all-start.3 = ((bf16[32,32,256]{2,1,0:T(8,128)(2,1)}), bf16[32,32,256]{2,1,0:T(8,128)(2,1)S(1)}, u32[]{:S(2)}, u32[]{:S(2)}) async-start(bf16[32,32,256]{2,1,0:T(8,128)(2,1)} %bitcast.13), calls=%async_computation.3 | async-start | bytes 1048576 | tf_op jit(solution)/shard_map/all_to_all | solution.py:126
Sparse Core Ops, SparseCore 0:
  180.2 50.5 all-gather.1
